TPU v7x, 32 devices: a whole 2x2x4 slice. The times are simulated.
32 devices in a mesh: ep: 16 (over z, y, x), tp: 2 (over core).
Axes of the slice: x: 2, y: 2, z: 4, core: 2. Of those that a mesh axis runs over, the one named last changes fastest.
Arguments:
- tokens: bfloat16 [256, 2048], P('ep'), may hold values from -6 to 6
- norm_gain: float32 [2048], replicated, may hold values from 0.1 to 1.9
- query_weight: bfloat16 [2048, 1024], P('ep', 'tp'), may hold values from -0.125 to 0.125
- key_weight: bfloat16 [2048, 1024], P('ep', 'tp'), may hold values from -0.125 to 0.125
- value_weight: bfloat16 [2048, 1024], P('ep', 'tp'), may hold values from -0.125 to 0.125
- outgate_weight: bfloat16 [2048, 1024], P('ep', 'tp'), may hold values from -0.125 to 0.125
- input_weight: bfloat16 [2048, 8], P('ep', 'tp'), may hold values from -0.125 to 0.125
- forget_weight: bfloat16 [2048, 8], P('ep', 'tp'), may hold values from -0.125 to 0.125
- forget_bias: float32 [8], P('tp'), may hold values from -1 to 5
- memory: float32 [256, 8, 128, 128], P('ep', 'tp'), may hold values from -2.4 to 2.4
- stabilizer: float32 [256, 8], P('ep', 'tp'), may hold values from -3 to 3
- head_gain: float32 [1024], P('tp'), may hold values from 0.1 to 1.9
- mix_weight: bfloat16 [1024, 2048], P('tp', 'ep'), may hold values from -0.1875 to 0.1875
- second_gain: float32 [2048], replicated, may hold values from 0.1 to 1.9
- route_experts: int32 [256, 4], P('ep'), may hold values from 0 to 15, all different within a row; in each aligned block of 16 rows (0 to 15, 16 to 31, ...) at most 8 rows name the same one
- route_weight: float32 [256, 4], P('ep'), may hold values from 0.1 to 1
- expert_gate: bfloat16 [16, 2048, 2048], P('ep', None, 'tp'), may hold values from -0.5 to 0.5
- expert_up: bfloat16 [16, 2048, 2048], P('ep', None, 'tp'), may hold values from -0.5 to 0.5
- expert_down: bfloat16 [16, 2048, 2048], P('ep', 'tp'), may hold values from -0.03125 to 0.03125
- dense_gate: bfloat16 [4096, 2048], P(('ep', 'tp')), may hold values from -0.125 to 0.125
- dense_up: bfloat16 [4096, 2048], P(('ep', 'tp')), may hold values from -0.125 to 0.125
- dense_down: bfloat16 [4096, 2048], P(('ep', 'tp')), may hold values from -0.09375 to 0.09375
- branch_scale: float32 [2048], replicated, may hold values from 0.3 to 1.5
Outputs:
- mixed: bfloat16 [256, 2048], P('ep', 'tp')
- memory_new: float32 [256, 8, 128, 128], P('ep', 'tp')
- stabilizer_new: float32 [256, 8], P('ep', 'tp')
Inputs may be any that keep to these rules, and one draw needn't show every extreme that they name: `route_experts`: each row names 4 different experts. Within each aligned block of 16 rows no expert is named by more than 8 rows, and in every draw some expert is named by exactly 8 rows of some block.
All inputs are finite; a program needn't handle non-finite values.
Results may differ from a plain program's by a relative error of at most 0.03.
Values may be sent and summed in bfloat16 or wider, within the bound.
A program may use at most 128 MiB of HBM per device.

v0:
```python
import jax
import jax.numpy as jnp
from jax import lax
from jax.sharding import PartitionSpec as P

norm_eps = 1e-05
clamp_limit = 7.0
sigmoid_slope = 1.702


def rms_scale(values, gain):
    mean_square = jnp.mean(values * values, axis=-1, keepdims=True)
    return values * lax.rsqrt(mean_square + norm_eps) * gain


def round_half(values):
    return lax.optimization_barrier(values.astype(jnp.bfloat16)).astype(jnp.float32)


def clamped_unit(gate_pre, up_pre):
    gate_clamped = jnp.minimum(gate_pre, clamp_limit)
    up_clamped = jnp.clip(up_pre, -clamp_limit, clamp_limit)
    return (
        (up_clamped + 1.0) * gate_clamped * jax.nn.sigmoid(sigmoid_slope * gate_clamped)
    ).astype(jnp.bfloat16)


def memory_step(projected, forget_bias, memory, stabilizer, head_gain):
    query_rows, key_rows, value_rows, outgate_rows, input_pre, forget_pre = projected
    sequences, head_count = stabilizer.shape
    head_size = memory.shape[-1]
    log_forget = jax.nn.log_sigmoid(forget_pre + forget_bias)
    stab_new = jnp.maximum(log_forget + stabilizer, input_pre)
    carried = jnp.exp(log_forget + stabilizer - stab_new)
    written = jnp.exp(input_pre - stab_new)
    query_heads = query_rows.astype(jnp.float32).reshape(sequences, head_count, head_size)
    key_heads = key_rows.astype(jnp.float32).reshape(
        sequences, head_count, head_size
    ) * head_size ** (-0.5)
    value_heads = value_rows.astype(jnp.float32).reshape(sequences, head_count, head_size)
    memory_new = (
        carried[:, :, None, None] * memory
        + written[:, :, None, None] * value_heads[:, :, :, None] * key_heads[:, :, None, :]
    )
    readout = jnp.einsum("bhvk,bhk->bhv", memory_new, query_heads, precision=lax.Precision.HIGHEST)
    out_gate = jax.nn.sigmoid(
        outgate_rows.astype(jnp.float32).reshape(sequences, head_count, head_size)
    )
    gated = (rms_scale(readout, head_gain.reshape(head_count, head_size)) * out_gate).astype(
        jnp.bfloat16
    )
    return (gated.reshape(sequences, head_count * head_size), memory_new, stab_new)


def expert_apply(rows, gate_weight, up_weight, down_weight):
    gate_pre = jnp.dot(rows, gate_weight, preferred_element_type=jnp.float32)
    up_pre = jnp.dot(rows, up_weight, preferred_element_type=jnp.float32)
    activity = clamped_unit(gate_pre, up_pre)
    return jnp.dot(activity, down_weight, preferred_element_type=jnp.float32).astype(jnp.bfloat16)


def slot_table(hit_mask, capacity):
    ranks = jnp.cumsum(hit_mask, axis=1) - 1.0
    slots = jnp.arange(capacity).astype(jnp.float32)
    return hit_mask[:, None, :] * (ranks[:, None, :] == slots[None, :, None]).astype(jnp.float32)


def body(
    tokens,
    norm_gain,
    query_weight,
    key_weight,
    value_weight,
    outgate_weight,
    input_weight,
    forget_weight,
    forget_bias,
    memory,
    stabilizer,
    head_gain,
    mix_weight,
    second_gain,
    route_experts,
    route_weight,
    expert_gate,
    expert_up,
    expert_down,
    dense_gate,
    dense_up,
    dense_down,
    branch_scale,
):
    sequences, model_width = tokens.shape
    ep_count = lax.axis_size("ep")
    tp_count = lax.axis_size("tp")
    part_width = model_width // tp_count
    top_count = route_experts.shape[1]
    expert_count = expert_gate.shape[0] * ep_count
    capacity = max(2, 2 * sequences * top_count // expert_count)
    inputs_float = tokens.astype(jnp.float32)
    normed = rms_scale(inputs_float, norm_gain).astype(jnp.bfloat16)
    weight_list = (
        query_weight,
        key_weight,
        value_weight,
        outgate_weight,
        input_weight,
        forget_weight,
    )
    columns = lax.all_to_all(normed, "ep", split_axis=1, concat_axis=0, tiled=True)
    joined = jnp.concatenate(weight_list, axis=1)
    summed_rows = lax.psum_scatter(
        jnp.dot(columns, joined, preferred_element_type=jnp.float32),
        "ep",
        scatter_dimension=0,
        tiled=True,
    )
    pieces = []
    lower = 0
    for weight in weight_list:
        pieces.append(summed_rows[:, lower : lower + weight.shape[1]])
        lower = lower + weight.shape[1]
    sums = tuple(pieces)
    projected = (
        sums[0].astype(jnp.bfloat16),
        sums[1].astype(jnp.bfloat16),
        sums[2].astype(jnp.bfloat16),
        sums[3].astype(jnp.bfloat16),
        sums[4],
        sums[5],
    )
    gated, memory_new, stab_new = memory_step(projected, forget_bias, memory, stabilizer, head_gain)
    partial_value = jnp.dot(
        gated,
        lax.all_gather(mix_weight, "ep", axis=1, tiled=True),
        preferred_element_type=jnp.float32,
    )
    attended = lax.psum(round_half(partial_value).astype(jnp.bfloat16), "tp").astype(jnp.float32)
    residual = (inputs_float + attended).astype(jnp.bfloat16)
    residual_float = residual.astype(jnp.float32)
    normed_second = rms_scale(residual_float, second_gain).astype(jnp.bfloat16)
    own_residual = lax.dynamic_slice_in_dim(
        residual_float, lax.axis_index("tp") * part_width, part_width, 1
    )
    matched = route_experts[:, :, None] == jnp.arange(expert_count)[None, None, :]
    hit_mask = jnp.any(matched, axis=1).astype(jnp.float32).T
    weights = jnp.sum(jnp.where(matched, route_weight[:, :, None], 0.0), axis=1).T
    select = slot_table(hit_mask, capacity)
    outgoing = jnp.einsum(
        "ecs,sd->ecd",
        select.astype(jnp.bfloat16),
        normed_second,
        preferred_element_type=jnp.float32,
    ).astype(jnp.bfloat16)
    received = lax.all_to_all(outgoing, "ep", split_axis=0, concat_axis=0, tiled=True)
    count = received.shape[1]
    partial_out = expert_apply(
        received.reshape(-1, model_width), expert_gate[0], expert_up[0], expert_down[0]
    )
    halves = lax.psum_scatter(
        partial_out.astype(jnp.float32).astype(jnp.bfloat16), "tp", scatter_dimension=1, tiled=True
    ).astype(jnp.float32)
    returned = lax.all_to_all(
        halves.reshape(ep_count, count, part_width).astype(jnp.bfloat16),
        "ep",
        split_axis=0,
        concat_axis=0,
        tiled=True,
    ).astype(jnp.float32)
    routed = jnp.einsum(
        "ecs,ecd->sd", select * weights[:, None, :], returned, precision=lax.Precision.HIGHEST
    )
    all_rows = lax.all_gather(normed_second, "ep", axis=0, tiled=True)
    gate_rows = jnp.einsum("fd,td->ft", dense_gate, all_rows, preferred_element_type=jnp.float32)
    lift_rows = jnp.einsum("fd,td->ft", dense_up, all_rows, preferred_element_type=jnp.float32)
    activity = (
        (jax.nn.silu(gate_rows) * lift_rows).astype(jnp.bfloat16).reshape(-1, ep_count, sequences)
    )
    down_parts = dense_down.reshape(-1, tp_count, part_width)
    term = jnp.einsum("fjs,fhd->jhsd", activity, down_parts, preferred_element_type=jnp.float32)
    branch = lax.psum_scatter(
        (term * branch_scale.reshape(1, tp_count, 1, part_width)).reshape(-1, part_width),
        ("ep", "tp"),
        scatter_dimension=0,
        tiled=True,
    )
    mixed = own_residual + routed + branch
    return (mixed.astype(jnp.bfloat16), memory_new, stab_new)


def solution(mesh):
    in_specs = (
        P("ep", None),
        P(),
        P("ep", "tp"),
        P("ep", "tp"),
        P("ep", "tp"),
        P("ep", "tp"),
        P("ep", "tp"),
        P("ep", "tp"),
        P("tp"),
        P("ep", "tp", None, None),
        P("ep", "tp"),
        P("tp"),
        P("tp", "ep"),
        P(),
        P("ep", None),
        P("ep", None),
        P("ep", None, "tp"),
        P("ep", None, "tp"),
        P("ep", "tp", None),
        P(("ep", "tp"), None),
        P(("ep", "tp"), None),
        P(("ep", "tp"), None),
        P(),
    )
    out_specs = (P("ep", "tp"), P("ep", "tp", None, None), P("ep", "tp"))
    return jax.shard_map(body, mesh=mesh, in_specs=in_specs, out_specs=out_specs, check_vma=False)
```

profile of v0, /device:TPU:0, one launch (start us, length us, event | category | flops | bytes accessed | tf_op | source)
XLA Modules:
  0.0 416.8 jit_solution(380059310604357217)
XLA Ops:
  7.2 1.0 fusion.48
  8.2 1.6 copy_bitcast_fusion
  9.8 8.3 %all-to-all-start = ((bf16[16,16,128]{2,0,1:T(8,128)(2,1)}), bf16[16,16,128]{2,0,1:T(8,128)(2,1)S(1)}, u32[]{:S(2)}, u32[]{:S(2)}) async-start(bf16[16,16,128]{2,0,1:T(8,128)(2,1)} %copy_bitcast_fusion), calls=%async_computation | async-start | bytes 131072 | tf_op jit(solution)/shard_map/all_to_all | solution.py:110
  18.2 0.8 copy.62
  19.8 1.2 concatenate.3
  21.0 4.7 %all-to-all-done = bf16[16,16,128]{2,0,1:T(8,128)(2,1)S(1)} async-done(((bf16[16,16,128]{2,0,1:T(8,128)(2,1)}), bf16[16,16,128]{2,0,1:T(8,128)(2,1)S(1)}, u32[]{:S(2)}, u32[]{:S(2)}) %all-to-all-start) | async-done | bytes 65568 | tf_op jit(solution)/shard_map/all_to_all | solution.py:110
  25.7 1.8 fusion.72
  28.8 77.2 %reduce-scatter.4.cloned.1.call-done = f32[16,2056]{1,0:T(8,128)} async-done(((f32[256,2056]{1,0:T(8,128)}), f32[16,2056]{1,0:T(8,128)}) %reduce-scatter.4.cloned.1.call-update) | async-done | bytes 131600 | tf_op jit(solution)/shard_map/reduce_scatter | solution.py:112
  106.0 0.9 convert.8
  107.1 0.9 subtract_exponential_fusion.1
  108.8 3.0 multiply_add_fusion
  111.8 2.0 copy-done.1
  113.8 3.3 fusion.73
  117.4 51.6 %all-gather.3.cloned.1.call-done = bf16[512,2048]{1,0:T(8,128)(2,1)} async-done(((bf16[512,128]{1,0:T(8,128)(2,1)}), bf16[512,2048]{1,0:T(8,128)(2,1)}) %all-gather.3.cloned.1.call-update) | async-done | bytes 2097168 | tf_op jit(solution)/shard_map/all_gather | solution.py:135
  169.0 2.6 convolution_convert_fusion.1
  171.8 15.9 %all-reduce.2.cloned.1.call-done = bf16[16,2048]{1,0:T(8,128)(2,1)} async-done(((bf16[16,2048]{1,0:T(8,128)(2,1)}), bf16[16,2048]{1,0:T(8,128)(2,1)}) %all-reduce.2.cloned.1.call-update) | async-done | bytes 65552 | tf_op jit(solution)/shard_map/psum | solution.py:138
  187.7 1.0 fusion.52
  188.7 0.9 multiply_convert_fusion
  189.7 1.1 convolution_convert_fusion
  190.7 6.8 %all-to-all-start.1 = ((bf16[16,8,2048]{2,1,0:T(8,128)(2,1)}), bf16[16,8,2048]{2,1,0:T(8,128)(2,1)S(1)}, u32[]{:S(2)}, u32[]{:S(2)}) async-start(bf16[16,8,2048]{2,1,0:T(8,128)(2,1)} %convolution_convert_fusion), calls=%async_computation.2 | async-start | bytes 1048576 | tf_op jit(solution)/shard_map/all_to_all | solution.py:155
  198.2 14.9 %all-to-all-done.1 = bf16[16,8,2048]{2,1,0:T(8,128)(2,1)S(1)} async-done(((bf16[16,8,2048]{2,1,0:T(8,128)(2,1)}), bf16[16,8,2048]{2,1,0:T(8,128)(2,1)S(1)}, u32[]{:S(2)}, u32[]{:S(2)}) %all-to-all-start.1) | async-done | bytes 524320 | tf_op jit(solution)/shard_map/all_to_all | solution.py:155
  213.1 2.9 fusion.12
  216.0 5.7 %fusion.6 = bf16[128,2048]{1,0:T(8,128)(2,1)} fusion(bf16[1,1024,2048]{2,1,0:T(8,128)(2,1)} %param.41, f32[128,1024]{1,0:T(8,128)S(1)} %fusion.12, bf16[1,2048,1024]{2,1,0:T(8,128)(2,1)} %param.40, bf16[16,8,2048]{2,1,0:T(8,128)(2,1)S(1)} %all-to-all-done.1), kind=kOutput, calls=%fused_computation.7 | convolution fusion | flops 1075183616 | bytes 9961472 | tf_op jit(solution)/shard_map/dot_general | solution.py:59
  221.9 35.4 %all-gather.5.cloned.1.call-done = bf16[256,2048]{1,0:T(8,128)(2,1)} async-done(((bf16[16,2048]{1,0:T(8,128)(2,1)}), bf16[256,2048]{1,0:T(8,128)(2,1)}) %all-gather.5.cloned.1.call-update) | async-done | bytes 1048592 | tf_op jit(solution)/shard_map/all_gather | solution.py:173
  257.3 1.7 convolution_bitcast_fusion.1
  258.9 1.7 fusion.28
  260.6 1.8 convolution_multiply_fusion
  262.4 3.8 reduce-scatter.6.cloned.1.call-done
  266.2 6.7 %all-to-all-start.2 = ((bf16[16,8,1024]{2,1,0:T(8,128)(2,1)}), bf16[16,8,1024]{2,1,0:T(8,128)(2,1)S(1)}, u32[]{:S(2)}, u32[]{:S(2)}) async-start(bf16[16,8,1024]{2,1,0:T(8,128)(2,1)} %bitcast.100), calls=%async_computation.4 | async-start | bytes 524288 | tf_op jit(solution)/shard_map/all_to_all | solution.py:163
  273.6 10.3 %all-to-all-done.2 = bf16[16,8,1024]{2,1,0:T(8,128)(2,1)S(1)} async-done(((bf16[16,8,1024]{2,1,0:T(8,128)(2,1)}), bf16[16,8,1024]{2,1,0:T(8,128)(2,1)S(1)}, u32[]{:S(2)}, u32[]{:S(2)}) %all-to-all-start.2) | async-done | bytes 262176 | tf_op jit(solution)/shard_map/all_to_all | solution.py:163
  284.0 124.0 %reduce-scatter.8.cloned.1.call-done = f32[16,1024]{1,0:T(8,128)} async-done(((f32[512,1024]{1,0:T(8,128)}), f32[16,1024]{1,0:T(8,128)}) %reduce-scatter.8.cloned.1.call-update) | async-done | bytes 65552 | tf_op jit(solution)/shard_map/reduce_scatter | solution.py:181
  407.9 2.0 fusion.31
  (64 shorter events, 4.9 us)
Async XLA Ops:
  7.2 250.1 %copy-start = (bf16[128,2048]{1,0:T(8,128)(2,1)S(1)}, bf16[128,2048]{1,0:T(8,128)(2,1)}, u32[]{:S(2)}) copy-start(bf16[128,2048]{1,0:T(8,128)(2,1)} %param.42) | copy-start | bytes 1572868
  7.2 21.1 %copy-start.8 = (f32[16,4]{0,1:T(4,128)S(1)}, f32[16,4]{0,1:T(4,128)}, u32[]{:S(2)}) copy-start(f32[16,4]{0,1:T(4,128)} %param.33) | copy-start | bytes 772
  7.2 21.2 %copy-start.7 = (s32[16,4]{0,1:T(4,128)S(1)}, s32[16,4]{0,1:T(4,128)}, u32[]{:S(2)}) copy-start(s32[16,4]{0,1:T(4,128)} %param.37) | copy-start | bytes 772
  7.2 99.9 %copy-start.11 = (f32[4]{0:T(128)S(1)}, f32[4]{0:T(128)}, u32[]{:S(2)}) copy-start(f32[4]{0:T(128)} %param.31) | copy-start | bytes 52
  9.8 15.9 %all-to-all-start = ((bf16[16,16,128]{2,0,1:T(8,128)(2,1)}), bf16[16,16,128]{2,0,1:T(8,128)(2,1)S(1)}, u32[]{:S(2)}, u32[]{:S(2)}) async-start(bf16[16,16,128]{2,0,1:T(8,128)(2,1)} %copy_bitcast_fusion), calls=%async_computation | async-start | bytes 131072 | tf_op jit(solution)/shard_map/all_to_all | solution.py:110
  18.2 87.9 %reduce-scatter.4.cloned.1.call-start = ((), (), s32[]{:S(2)}) async-start(), calls=%async_computation.6 | async-start | bytes 2367488 | tf_op jit(solution)/shard_map/reduce_scatter | solution.py:112
  27.5 141.5 %all-gather.3.cloned.1.call-start = ((), (), s32[]{:S(2)}) async-start(), calls=%async_computation.7 | async-start | bytes 2228224 | tf_op jit(solution)/shard_map/all_gather | solution.py:135
  28.3 159.5 %all-reduce.2.cloned.1.call-start = ((), (), s32[]{:S(2)}) async-start(), calls=%async_computation.8 | async-start | bytes 131072 | tf_op jit(solution)/shard_map/psum | solution.py:138
  111.8 2.0 copy-start.1
  113.8 3.5 copy-start.9
  113.8 73.9 %copy-start.2 = (bf16[16,2048]{1,0:T(8,128)(2,1)S(1)}, bf16[16,2048]{1,0:T(8,128)(2,1)}, u32[]{:S(2)}) copy-start(bf16[16,2048]{1,0:T(8,128)(2,1)} %param.23) | copy-start | bytes 196612
  113.8 74.9 %copy-start.5 = (f32[2048]{0:T(1024)S(1)}, f32[2048]{0:T(1024)}, u32[]{:S(2)}) copy-start(f32[2048]{0:T(1024)} %param.36) | copy-start | bytes 24580
  189.6 8.0 %copy-start.3 = (bf16[16,2048]{1,0:T(8,128)(2,1)}, bf16[16,2048]{1,0:T(8,128)(2,1)S(1)}, u32[]{:S(2)}) copy-start(bf16[16,2048]{1,0:T(8,128)(2,1)S(1)} %multiply_convert_fusion) | copy-start | bytes 196612
  190.7 22.3 %all-to-all-start.1 = ((bf16[16,8,2048]{2,1,0:T(8,128)(2,1)}), bf16[16,8,2048]{2,1,0:T(8,128)(2,1)S(1)}, u32[]{:S(2)}, u32[]{:S(2)}) async-start(bf16[16,8,2048]{2,1,0:T(8,128)(2,1)} %convolution_convert_fusion), calls=%async_computation.2 | async-start | bytes 1048576 | tf_op jit(solution)/shard_map/all_to_all | solution.py:155
  197.6 59.7 %all-gather.5.cloned.1.call-start = ((), (), s32[]{:S(2)}) async-start(), calls=%async_computation.10 | async-start | bytes 1114112 | tf_op jit(solution)/shard_map/all_gather | solution.py:173
  198.2 68.0 %reduce-scatter.6.cloned.1.call-start = ((), (), s32[]{:S(2)}) async-start(), calls=%async_computation.9 | async-start | bytes 786432 | tf_op jit(solution)/shard_map/reduce_scatter | solution.py:160
  216.0 5.8 %copy-start.6 = (f32[2048]{0:T(1024)S(1)}, f32[2048]{0:T(1024)}, u32[]{:S(2)}) copy-start(f32[2048]{0:T(1024)} %param.45) | copy-start | bytes 24580
  216.0 43.0 %copy-start.12 = (bf16[128,2048]{1,0:T(8,128)(2,1)S(1)}, bf16[128,2048]{1,0:T(8,128)(2,1)}, u32[]{:S(2)}) copy-start(bf16[128,2048]{1,0:T(8,128)(2,1)} %param.43) | copy-start | bytes 1572868
  221.7 38.9 %copy-start.4 = (bf16[128,2048]{1,0:T(8,128)(2,1)S(1)}, bf16[128,2048]{1,0:T(8,128)(2,1)}, u32[]{:S(2)}) copy-start(bf16[128,2048]{1,0:T(8,128)(2,1)} %param.44) | copy-start | bytes 1572868
  221.8 186.2 %reduce-scatter.8.cloned.1.call-start = ((), (), s32[]{:S(2)}) async-start(), calls=%async_computation.11 | async-start | bytes 2162688 | tf_op jit(solution)/shard_map/reduce_scatter | solution.py:181
  221.8 51.1 %copy-start.10 = (f32[16,4]{0,1:T(4,128)S(1)}, f32[16,4]{0,1:T(4,128)}, u32[]{:S(2)}) copy-start(f32[16,4]{0,1:T(4,128)} %param.38) | copy-start | bytes 772
  266.2 17.8 %all-to-all-start.2 = ((bf16[16,8,1024]{2,1,0:T(8,128)(2,1)}), bf16[16,8,1024]{2,1,0:T(8,128)(2,1)S(1)}, u32[]{:S(2)}, u32[]{:S(2)}) async-start(bf16[16,8,1024]{2,1,0:T(8,128)(2,1)} %bitcast.100), calls=%async_computation.4 | async-start | bytes 524288 | tf_op jit(solution)/shard_map/all_to_all | solution.py:163
Sparse Core Ops, SparseCore 0:
  27.6 78.3 reduce-scatter.3
  108.7 60.2 all-gather.2
  171.8 15.9 all-reduce.1
  200.8 56.3 all-gather.4
  259.4 6.7 reduce-scatter.5
  268.3 139.6 reduce-scatter.7
where the time goes:
time: 418 us; the launch traced here: 417 us
  waiting for transfers between devices  339 us (81%)
  matrix products  24.5 us (6%)
  starting transfers between devices  22.1 us (5%)
  between operations  14.4 us (3%)
  other arithmetic  10.8 us (3%)
  local copies, waits for them, and re-layouts  5.91 us (1%)
    reduce_scatter x1, waiting for transfers between devices, body(): lax.psum_scatter((term * branch_scale.reshape(1, tp_count, 1, part_width)...  124 us
    reduce_scatter x1, waiting for transfers between devices, body(): lax.psum_scatter(jnp.dot(columns, joined, preferred_element_type=jnp.floa...  77.2 us
    all_gather x1, waiting for transfers between devices, body(): lax.all_gather(mix_weight, 'ep', axis=1, tiled=True)  51.6 us
    all_gather x1, waiting for transfers between devices, body(): all_rows = lax.all_gather(normed_second, 'ep', axis=0, tiled=True)  35.4 us
    psum x1, waiting for transfers between devices, body(): lax.psum(round_half(partial_value).astype(jnp.bfloat16), 'tp')  15.9 us
    all_to_all x1, waiting for transfers between devices, body(): lax.all_to_all(outgoing, 'ep', split_axis=0, concat_axis=0, tiled=True)  14.9 us
    all_to_all x1, waiting for transfers between devices, body(): lax.all_to_all(halves.reshape(ep_count, count, part_width).astype(jnp.bfl...  10.3 us
  transfers between devices with their start and end apart: 9, of which 9 were waited for; matrix products, arithmetic and copies ran while one was open for 7% of the time, Pallas kernels for 0%

commit v1 on v0

--- a/solution.py
+++ b/solution.py
@@ -170,7 +170,21 @@
     routed = jnp.einsum(
         "ecs,ecd->sd", select * weights[:, None, :], returned, precision=lax.Precision.HIGHEST
     )
-    all_rows = lax.all_gather(normed_second, "ep", axis=0, tiled=True)
+    ways, here, turn = (lax.axis_size("ep"), lax.axis_index("ep"), normed_second.shape[0])
+    shape = [n * ways if d == 0 else n for d, n in enumerate(normed_second.shape)]
+    full = lax.dynamic_update_slice_in_dim(
+        jnp.zeros(shape, normed_second.dtype), normed_second, here * turn, axis=0
+    )
+    going_up = going_down = normed_second
+    for far in range(1, ways // 2 + 1):
+        going_up = lax.ppermute(going_up, "ep", [(d, (d + 1) % ways) for d in range(ways)])
+        full = lax.dynamic_update_slice_in_dim(full, going_up, (here - far) % ways * turn, axis=0)
+        if 2 * far < ways:
+            going_down = lax.ppermute(going_down, "ep", [(d, (d - 1) % ways) for d in range(ways)])
+            full = lax.dynamic_update_slice_in_dim(
+                full, going_down, (here + far) % ways * turn, axis=0
+            )
+    all_rows = full
     gate_rows = jnp.einsum("fd,td->ft", dense_gate, all_rows, preferred_element_type=jnp.float32)
     lift_rows = jnp.einsum("fd,td->ft", dense_up, all_rows, preferred_element_type=jnp.float32)
     activity = (

time: 418 us -> 426 us (1.019)
  starting transfers between devices: 22.1 us -> 58.3 us
  waiting for transfers between devices: 339 us -> 313 us
    ppermute x0 -> x15, starting transfers between devices: none -> 39.5 us  [the longest x7 35.8 us: body(): lax.ppermute(going_down, 'ep', [(d, (d - 1) % ways) for d in range(ways)])]
    all_gather x1 -> x0, waiting for transfers between devices: 35.4 us -> none  [body(): all_rows = lax.all_gather(normed_second, 'ep', axis=0, tiled=True)]
    ppermute x0 -> x15, waiting for transfers between devices: none -> 21.9 us  [the longest x8 21.9 us: body(): lax.ppermute(going_up, 'ep', [(d, (d + 1) % ways) for d in range(ways)])]
    all_to_all x1, waiting for transfers between devices: 14.9 us -> 0.01 us  [body(): lax.all_to_all(outgoing, 'ep', split_axis=0, concat_axis=0, tiled=True)]
  transfers between devices with their start and end apart: 9 -> 23, of which waited for: 9 -> 13; matrix products, arithmetic and copies ran while one was open for 7% -> 6% of each run, Pallas kernels for 0% -> 0%
where the time goes in v1:
time: 426 us; the launch traced here: 425 us
  waiting for transfers between devices  313 us (73%)
  starting transfers between devices  58.3 us (14%)
  matrix products  22 us (5%)
  between operations  14.6 us (3%)
  other arithmetic  10.7 us (3%)
  local copies, waits for them, and re-layouts  6.18 us (1%)
    reduce_scatter x1, waiting for transfers between devices, body(): lax.psum_scatter((term * branch_scale.reshape(1, tp_count, 1, part_width)...  124 us
    reduce_scatter x1, waiting for transfers between devices, body(): lax.psum_scatter(jnp.dot(columns, joined, preferred_element_type=jnp.floa...  77.3 us
    all_gather x1, waiting for transfers between devices, body(): lax.all_gather(mix_weight, 'ep', axis=1, tiled=True)  51.6 us
    ppermute x7, starting transfers between devices, body(): lax.ppermute(going_down, 'ep', [(d, (d - 1) % ways) for d in range(ways)])  35.8 us
    ppermute x8, waiting for transfers between devices, body(): lax.ppermute(going_up, 'ep', [(d, (d + 1) % ways) for d in range(ways)])  21.9 us
    psum x1, waiting for transfers between devices, body(): lax.psum(round_half(partial_value).astype(jnp.bfloat16), 'tp')  15.5 us
    all_to_all x1, waiting for transfers between devices, body(): lax.all_to_all(halves.reshape(ep_count, count, part_width).astype(jnp.bfl...  10.3 us
  transfers between devices with their start and end apart: 23, of which 13 were waited for; matrix products, arithmetic and copies ran while one was open for 6% of the time, Pallas kernels for 0%

profile of v1, /device:TPU:0, one launch (start us, length us, event | category | flops | bytes accessed | tf_op | source)
XLA Modules:
  0.0 424.7 jit_solution(10314846912321315128)
XLA Ops:
  9.8 8.3 %all-to-all-start = ((bf16[16,16,128]{2,0,1:T(8,128)(2,1)}), bf16[16,16,128]{2,0,1:T(8,128)(2,1)S(1)}, u32[]{:S(2)}, u32[]{:S(2)}) async-start(bf16[16,16,128]{2,0,1:T(8,128)(2,1)} %copy_bitcast_fusion), calls=%async_computation | async-start | bytes 131072 | tf_op jit(solution)/shard_map/all_to_all | solution.py:110
  21.0 4.7 %all-to-all-done = bf16[16,16,128]{2,0,1:T(8,128)(2,1)S(1)} async-done(((bf16[16,16,128]{2,0,1:T(8,128)(2,1)}), bf16[16,16,128]{2,0,1:T(8,128)(2,1)S(1)}, u32[]{:S(2)}, u32[]{:S(2)}) %all-to-all-start) | async-done | bytes 65568 | tf_op jit(solution)/shard_map/all_to_all | solution.py:110
  28.8 77.3 %reduce-scatter.4.cloned.1.call-done = f32[16,2056]{1,0:T(8,128)} async-done(((f32[256,2056]{1,0:T(8,128)}), f32[16,2056]{1,0:T(8,128)}) %reduce-scatter.4.cloned.1.call-update) | async-done | bytes 131600 | tf_op jit(solution)/shard_map/reduce_scatter | solution.py:112
  108.9 3.0 multiply_add_fusion
  111.9 2.0 copy-done.1
  113.9 3.4 fusion.71
  117.5 51.6 %all-gather.2.cloned.1.call-done = bf16[512,2048]{1,0:T(8,128)(2,1)} async-done(((bf16[512,128]{1,0:T(8,128)(2,1)}), bf16[512,2048]{1,0:T(8,128)(2,1)}) %all-gather.2.cloned.1.call-update) | async-done | bytes 2097168 | tf_op jit(solution)/shard_map/all_gather | solution.py:135
  169.1 2.6 convolution_convert_fusion.1
  172.3 15.5 %all-reduce.2.cloned.1.call-done = bf16[16,2048]{1,0:T(8,128)(2,1)} async-done(((bf16[16,2048]{1,0:T(8,128)(2,1)}), bf16[16,2048]{1,0:T(8,128)(2,1)}) %all-reduce.2.cloned.1.call-update) | async-done | bytes 65552 | tf_op jit(solution)/shard_map/psum | solution.py:138
  189.9 1.8 collective-permute-start
  191.7 3.8 collective-permute-start.1
  196.6 3.6 all-to-all-start.1
  200.2 1.9 collective-permute-start.2
  202.1 3.8 collective-permute-start.3
  206.0 10.2 %collective-permute-done.2 = bf16[16,2048]{1,0:T(8,128)(2,1)S(1)} collective-permute-done((bf16[16,2048]{1,0:T(8,128)(2,1)S(1)}, bf16[16,2048]{1,0:T(8,128)(2,1)S(1)}, u32[]{:S(2)}, u32[]{:S(2)}) %collective-permute-start.2) | collective-permute-done | bytes 65568 | tf_op jit(solution)/shard_map/ppermute | solution.py:180
  216.2 5.6 %collective-permute-start.5 = (bf16[16,2048]{1,0:T(8,128)(2,1)S(1)}, bf16[16,2048]{1,0:T(8,128)(2,1)S(1)}, u32[]{:S(2)}, u32[]{:S(2)}) collective-permute-start(bf16[16,2048]{1,0:T(8,128)(2,1)S(1)} %collective-permute-done.3), channel_id=1, source_target_pairs={{0,30},{2,0},{4,2},{6,4},{8,6},{10,8},{12,10},{14,12},{16,14},{18,... | collective-permute-start | bytes 196616 | tf_op jit(solution)/shard_map/ppermute | solution.py:183
  221.9 2.2 collective-permute-done.4
  224.1 5.6 %collective-permute-start.7 = (bf16[16,2048]{1,0:T(8,128)(2,1)S(1)}, bf16[16,2048]{1,0:T(8,128)(2,1)S(1)}, u32[]{:S(2)}, u32[]{:S(2)}) collective-permute-start(bf16[16,2048]{1,0:T(8,128)(2,1)S(1)} %collective-permute-done.5), channel_id=1, source_target_pairs={{0,30},{2,0},{4,2},{6,4},{8,6},{10,8},{12,10},{14,12},{16,14},{18,... | collective-permute-start | bytes 196616 | tf_op jit(solution)/shard_map/ppermute | solution.py:183
  229.7 2.3 collective-permute-done.6
  232.0 5.6 %collective-permute-start.9 = (bf16[16,2048]{1,0:T(8,128)(2,1)S(1)}, bf16[16,2048]{1,0:T(8,128)(2,1)S(1)}, u32[]{:S(2)}, u32[]{:S(2)}) collective-permute-start(bf16[16,2048]{1,0:T(8,128)(2,1)S(1)} %collective-permute-done.7), channel_id=1, source_target_pairs={{0,30},{2,0},{4,2},{6,4},{8,6},{10,8},{12,10},{14,12},{16,14},{18,... | collective-permute-start | bytes 196616 | tf_op jit(solution)/shard_map/ppermute | solution.py:183
  237.7 2.2 collective-permute-done.8
  239.9 5.6 %collective-permute-start.11 = (bf16[16,2048]{1,0:T(8,128)(2,1)S(1)}, bf16[16,2048]{1,0:T(8,128)(2,1)S(1)}, u32[]{:S(2)}, u32[]{:S(2)}) collective-permute-start(bf16[16,2048]{1,0:T(8,128)(2,1)S(1)} %collective-permute-done.9), channel_id=1, source_target_pairs={{0,30},{2,0},{4,2},{6,4},{8,6},{10,8},{12,10},{14,12},{16,14},{18,... | collective-permute-start | bytes 196616 | tf_op jit(solution)/shard_map/ppermute | solution.py:183
  245.5 2.2 collective-permute-done.10
  247.8 5.6 %collective-permute-start.13 = (bf16[16,2048]{1,0:T(8,128)(2,1)S(1)}, bf16[16,2048]{1,0:T(8,128)(2,1)S(1)}, u32[]{:S(2)}, u32[]{:S(2)}) collective-permute-start(bf16[16,2048]{1,0:T(8,128)(2,1)S(1)} %collective-permute-done.11), channel_id=1, source_target_pairs={{0,30},{2,0},{4,2},{6,4},{8,6},{10,8},{12,10},{14,12},{16,14},{18,... | collective-permute-start | bytes 196616 | tf_op jit(solution)/shard_map/ppermute | solution.py:183
  253.4 2.7 collective-permute-done.12
  256.2 2.9 fusion.12
  259.1 5.7 %fusion.6 = bf16[128,2048]{1,0:T(8,128)(2,1)} fusion(bf16[1,1024,2048]{2,1,0:T(8,128)(2,1)} %param.41, f32[128,1024]{1,0:T(8,128)S(1)} %fusion.12, bf16[1,2048,1024]{2,1,0:T(8,128)(2,1)} %param.40, bf16[16,8,2048]{2,1,0:T(8,128)(2,1)S(1)} %all-to-all-done.1), kind=kOutput, calls=%fused_computation.7 | convolution fusion | flops 1075183616 | bytes 9961472 | tf_op jit(solution)/shard_map/dot_general | solution.py:59
  267.6 6.7 %reduce-scatter.6.cloned.1.call-done = bf16[128,1024]{1,0:T(8,128)(2,1)} async-done(((bf16[128,2048]{1,0:T(8,128)(2,1)}), bf16[128,1024]{1,0:T(8,128)(2,1)}) %reduce-scatter.6.cloned.1.call-update) | async-done | bytes 262160 | tf_op jit(solution)/shard_map/reduce_scatter | solution.py:160
  274.3 6.7 %all-to-all-start.2 = ((bf16[16,8,1024]{2,1,0:T(8,128)(2,1)}), bf16[16,8,1024]{2,1,0:T(8,128)(2,1)S(1)}, u32[]{:S(2)}, u32[]{:S(2)}) async-start(bf16[16,8,1024]{2,1,0:T(8,128)(2,1)} %bitcast.96), calls=%async_computation.4 | async-start | bytes 524288 | tf_op jit(solution)/shard_map/all_to_all | solution.py:163
  281.8 10.3 %all-to-all-done.2 = bf16[16,8,1024]{2,1,0:T(8,128)(2,1)S(1)} async-done(((bf16[16,8,1024]{2,1,0:T(8,128)(2,1)}), bf16[16,8,1024]{2,1,0:T(8,128)(2,1)S(1)}, u32[]{:S(2)}, u32[]{:S(2)}) %all-to-all-start.2) | async-done | bytes 262176 | tf_op jit(solution)/shard_map/all_to_all | solution.py:163
  292.1 124.1 %reduce-scatter.8.cloned.1.call-done = f32[16,1024]{1,0:T(8,128)} async-done(((f32[512,1024]{1,0:T(8,128)}), f32[16,1024]{1,0:T(8,128)}) %reduce-scatter.8.cloned.1.call-update) | async-done | bytes 65552 | tf_op jit(solution)/shard_map/reduce_scatter | solution.py:195
  416.2 2.0 fusion.29
  (105 shorter events, 18.4 us)
Async XLA Ops:
  7.2 257.8 %copy-start = (bf16[128,2048]{1,0:T(8,128)(2,1)S(1)}, bf16[128,2048]{1,0:T(8,128)(2,1)}, u32[]{:S(2)}) copy-start(bf16[128,2048]{1,0:T(8,128)(2,1)} %param.42) | copy-start | bytes 1572868
  7.2 21.1 %copy-start.7 = (f32[16,4]{0,1:T(4,128)S(1)}, f32[16,4]{0,1:T(4,128)}, u32[]{:S(2)}) copy-start(f32[16,4]{0,1:T(4,128)} %param.33) | copy-start | bytes 772
  7.2 21.2 %copy-start.6 = (s32[16,4]{0,1:T(4,128)S(1)}, s32[16,4]{0,1:T(4,128)}, u32[]{:S(2)}) copy-start(s32[16,4]{0,1:T(4,128)} %param.37) | copy-start | bytes 772
  7.2 100.0 %copy-start.10 = (f32[4]{0:T(128)S(1)}, f32[4]{0:T(128)}, u32[]{:S(2)}) copy-start(f32[4]{0:T(128)} %param.31) | copy-start | bytes 52
  9.8 15.9 %all-to-all-start = ((bf16[16,16,128]{2,0,1:T(8,128)(2,1)}), bf16[16,16,128]{2,0,1:T(8,128)(2,1)S(1)}, u32[]{:S(2)}, u32[]{:S(2)}) async-start(bf16[16,16,128]{2,0,1:T(8,128)(2,1)} %copy_bitcast_fusion), calls=%async_computation | async-start | bytes 131072 | tf_op jit(solution)/shard_map/all_to_all | solution.py:110
  18.2 88.0 %reduce-scatter.4.cloned.1.call-start = ((), (), s32[]{:S(2)}) async-start(), calls=%async_computation.6 | async-start | bytes 2367488 | tf_op jit(solution)/shard_map/reduce_scatter | solution.py:112
  27.5 141.6 %all-gather.2.cloned.1.call-start = ((), (), s32[]{:S(2)}) async-start(), calls=%async_computation.7 | async-start | bytes 2228224 | tf_op jit(solution)/shard_map/all_gather | solution.py:135
  28.3 159.5 %all-reduce.2.cloned.1.call-start = ((), (), s32[]{:S(2)}) async-start(), calls=%async_computation.8 | async-start | bytes 131072 | tf_op jit(solution)/shard_map/psum | solution.py:138
  113.9 58.2 %copy-start.5 = (f32[2048]{0:T(1024)S(1)}, f32[2048]{0:T(1024)}, u32[]{:S(2)}) copy-start(f32[2048]{0:T(1024)} %param.45) | copy-start | bytes 24580
  113.9 73.9 %copy-start.2 = (bf16[16,2048]{1,0:T(8,128)(2,1)S(1)}, bf16[16,2048]{1,0:T(8,128)(2,1)}, u32[]{:S(2)}) copy-start(bf16[16,2048]{1,0:T(8,128)(2,1)} %param.23) | copy-start | bytes 196612
  113.9 75.0 %copy-start.4 = (f32[2048]{0:T(1024)S(1)}, f32[2048]{0:T(1024)}, u32[]{:S(2)}) copy-start(f32[2048]{0:T(1024)} %param.36) | copy-start | bytes 24580
  189.9 10.4 %collective-permute-start = (bf16[16,2048]{1,0:T(8,128)(2,1)S(1)}, bf16[16,2048]{1,0:T(8,128)(2,1)S(1)}, u32[]{:S(2)}, u32[]{:S(2)}) collective-permute-start(bf16[16,2048]{1,0:T(8,128)(2,1)S(1)} %get-tuple-element.16), channel_id=1, source_target_pairs={{0,2},{2,4},{4,6},{6,8},{8,10},{10,12},{12,14},{14,16},{16,18},{18... | collective-permute-start | bytes 196616 | tf_op jit(solution)/shard_map/ppermute | solution.py:180
  191.7 10.4 %collective-permute-start.1 = (bf16[16,2048]{1,0:T(8,128)(2,1)S(1)}, bf16[16,2048]{1,0:T(8,128)(2,1)S(1)}, u32[]{:S(2)}, u32[]{:S(2)}) collective-permute-start(bf16[16,2048]{1,0:T(8,128)(2,1)S(1)} %get-tuple-element.16), channel_id=1, source_target_pairs={{0,30},{2,0},{4,2},{6,4},{8,6},{10,8},{12,10},{14,12},{16,14},{18,... | collective-permute-start | bytes 196616 | tf_op jit(solution)/shard_map/ppermute | solution.py:183
  196.6 59.6 %all-to-all-start.1 = ((bf16[16,8,2048]{2,1,0:T(8,128)(2,1)}), bf16[16,8,2048]{2,1,0:T(8,128)(2,1)S(1)}, u32[]{:S(2)}, u32[]{:S(2)}) async-start(bf16[16,8,2048]{2,1,0:T(8,128)(2,1)} %convolution_convert_fusion), calls=%async_computation.2 | async-start | bytes 1048576 | tf_op jit(solution)/shard_map/all_to_all | solution.py:155
  200.2 74.1 %reduce-scatter.6.cloned.1.call-start = ((), (), s32[]{:S(2)}) async-start(), calls=%async_computation.9 | async-start | bytes 786432 | tf_op jit(solution)/shard_map/reduce_scatter | solution.py:160
  200.2 16.0 %collective-permute-start.2 = (bf16[16,2048]{1,0:T(8,128)(2,1)S(1)}, bf16[16,2048]{1,0:T(8,128)(2,1)S(1)}, u32[]{:S(2)}, u32[]{:S(2)}) collective-permute-start(bf16[16,2048]{1,0:T(8,128)(2,1)S(1)} %collective-permute-done), channel_id=1, source_target_pairs={{0,2},{2,4},{4,6},{6,8},{8,10},{10,12},{12,14},{14,16},{16,18},{18... | collective-permute-start | bytes 196616 | tf_op jit(solution)/shard_map/ppermute | solution.py:180
  202.1 14.1 %collective-permute-start.3 = (bf16[16,2048]{1,0:T(8,128)(2,1)S(1)}, bf16[16,2048]{1,0:T(8,128)(2,1)S(1)}, u32[]{:S(2)}, u32[]{:S(2)}) collective-permute-start(bf16[16,2048]{1,0:T(8,128)(2,1)S(1)} %collective-permute-done.1), channel_id=1, source_target_pairs={{0,30},{2,0},{4,2},{6,4},{8,6},{10,8},{12,10},{14,12},{16,14},{18,... | collective-permute-start | bytes 196616 | tf_op jit(solution)/shard_map/ppermute | solution.py:183
  216.2 7.9 %collective-permute-start.4 = (bf16[16,2048]{1,0:T(8,128)(2,1)S(1)}, bf16[16,2048]{1,0:T(8,128)(2,1)S(1)}, u32[]{:S(2)}, u32[]{:S(2)}) collective-permute-start(bf16[16,2048]{1,0:T(8,128)(2,1)S(1)} %collective-permute-done.2), channel_id=1, source_target_pairs={{0,2},{2,4},{4,6},{6,8},{8,10},{10,12},{12,14},{14,16},{16,18},{18... | collective-permute-start | bytes 196616 | tf_op jit(solution)/shard_map/ppermute | solution.py:180
  216.2 7.9 %collective-permute-start.5 = (bf16[16,2048]{1,0:T(8,128)(2,1)S(1)}, bf16[16,2048]{1,0:T(8,128)(2,1)S(1)}, u32[]{:S(2)}, u32[]{:S(2)}) collective-permute-start(bf16[16,2048]{1,0:T(8,128)(2,1)S(1)} %collective-permute-done.3), channel_id=1, source_target_pairs={{0,30},{2,0},{4,2},{6,4},{8,6},{10,8},{12,10},{14,12},{16,14},{18,... | collective-permute-start | bytes 196616 | tf_op jit(solution)/shard_map/ppermute | solution.py:183
  224.1 8.0 %collective-permute-start.6 = (bf16[16,2048]{1,0:T(8,128)(2,1)S(1)}, bf16[16,2048]{1,0:T(8,128)(2,1)S(1)}, u32[]{:S(2)}, u32[]{:S(2)}) collective-permute-start(bf16[16,2048]{1,0:T(8,128)(2,1)S(1)} %collective-permute-done.4), channel_id=1, source_target_pairs={{0,2},{2,4},{4,6},{6,8},{8,10},{10,12},{12,14},{14,16},{16,18},{18... | collective-permute-start | bytes 196616 | tf_op jit(solution)/shard_map/ppermute | solution.py:180
  224.1 8.0 %collective-permute-start.7 = (bf16[16,2048]{1,0:T(8,128)(2,1)S(1)}, bf16[16,2048]{1,0:T(8,128)(2,1)S(1)}, u32[]{:S(2)}, u32[]{:S(2)}) collective-permute-start(bf16[16,2048]{1,0:T(8,128)(2,1)S(1)} %collective-permute-done.5), channel_id=1, source_target_pairs={{0,30},{2,0},{4,2},{6,4},{8,6},{10,8},{12,10},{14,12},{16,14},{18,... | collective-permute-start | bytes 196616 | tf_op jit(solution)/shard_map/ppermute | solution.py:183
  232.0 7.9 %collective-permute-start.8 = (bf16[16,2048]{1,0:T(8,128)(2,1)S(1)}, bf16[16,2048]{1,0:T(8,128)(2,1)S(1)}, u32[]{:S(2)}, u32[]{:S(2)}) collective-permute-start(bf16[16,2048]{1,0:T(8,128)(2,1)S(1)} %collective-permute-done.6), channel_id=1, source_target_pairs={{0,2},{2,4},{4,6},{6,8},{8,10},{10,12},{12,14},{14,16},{16,18},{18... | collective-permute-start | bytes 196616 | tf_op jit(solution)/shard_map/ppermute | solution.py:180
  232.0 7.9 %collective-permute-start.9 = (bf16[16,2048]{1,0:T(8,128)(2,1)S(1)}, bf16[16,2048]{1,0:T(8,128)(2,1)S(1)}, u32[]{:S(2)}, u32[]{:S(2)}) collective-permute-start(bf16[16,2048]{1,0:T(8,128)(2,1)S(1)} %collective-permute-done.7), channel_id=1, source_target_pairs={{0,30},{2,0},{4,2},{6,4},{8,6},{10,8},{12,10},{14,12},{16,14},{18,... | collective-permute-start | bytes 196616 | tf_op jit(solution)/shard_map/ppermute | solution.py:183
  239.9 7.9 %collective-permute-start.10 = (bf16[16,2048]{1,0:T(8,128)(2,1)S(1)}, bf16[16,2048]{1,0:T(8,128)(2,1)S(1)}, u32[]{:S(2)}, u32[]{:S(2)}) collective-permute-start(bf16[16,2048]{1,0:T(8,128)(2,1)S(1)} %collective-permute-done.8), channel_id=1, source_target_pairs={{0,2},{2,4},{4,6},{6,8},{8,10},{10,12},{12,14},{14,16},{16,18},{18... | collective-permute-start | bytes 196616 | tf_op jit(solution)/shard_map/ppermute | solution.py:180
  239.9 7.9 %collective-permute-start.11 = (bf16[16,2048]{1,0:T(8,128)(2,1)S(1)}, bf16[16,2048]{1,0:T(8,128)(2,1)S(1)}, u32[]{:S(2)}, u32[]{:S(2)}) collective-permute-start(bf16[16,2048]{1,0:T(8,128)(2,1)S(1)} %collective-permute-done.9), channel_id=1, source_target_pairs={{0,30},{2,0},{4,2},{6,4},{8,6},{10,8},{12,10},{14,12},{16,14},{18,... | collective-permute-start | bytes 196616 | tf_op jit(solution)/shard_map/ppermute | solution.py:183
  247.7 8.4 %collective-permute-start.12 = (bf16[16,2048]{1,0:T(8,128)(2,1)S(1)}, bf16[16,2048]{1,0:T(8,128)(2,1)S(1)}, u32[]{:S(2)}, u32[]{:S(2)}) collective-permute-start(bf16[16,2048]{1,0:T(8,128)(2,1)S(1)} %collective-permute-done.10), channel_id=1, source_target_pairs={{0,2},{2,4},{4,6},{6,8},{8,10},{10,12},{12,14},{14,16},{16,18},{18... | collective-permute-start | bytes 196616 | tf_op jit(solution)/shard_map/ppermute | solution.py:180
  247.8 8.4 %collective-permute-start.13 = (bf16[16,2048]{1,0:T(8,128)(2,1)S(1)}, bf16[16,2048]{1,0:T(8,128)(2,1)S(1)}, u32[]{:S(2)}, u32[]{:S(2)}) collective-permute-start(bf16[16,2048]{1,0:T(8,128)(2,1)S(1)} %collective-permute-done.11), channel_id=1, source_target_pairs={{0,30},{2,0},{4,2},{6,4},{8,6},{10,8},{12,10},{14,12},{16,14},{18,... | collective-permute-start | bytes 196616 | tf_op jit(solution)/shard_map/ppermute | solution.py:183
  256.1 8.8 %collective-permute-start.14 = (bf16[16,2048]{1,0:T(8,128)(2,1)S(1)}, bf16[16,2048]{1,0:T(8,128)(2,1)S(1)}, u32[]{:S(2)}, u32[]{:S(2)}) collective-permute-start(bf16[16,2048]{1,0:T(8,128)(2,1)S(1)} %collective-permute-done.12), channel_id=1, source_target_pairs={{0,2},{2,4},{4,6},{6,8},{8,10},{10,12},{12,14},{14,16},{16,18},{18... | collective-permute-start | bytes 196616 | tf_op jit(solution)/shard_map/ppermute | solution.py:180
  259.1 6.3 %copy-start.11 = (bf16[128,2048]{1,0:T(8,128)(2,1)S(1)}, bf16[128,2048]{1,0:T(8,128)(2,1)}, u32[]{:S(2)}) copy-start(bf16[128,2048]{1,0:T(8,128)(2,1)} %param.43) | copy-start | bytes 1572868
  264.9 151.4 %reduce-scatter.8.cloned.1.call-start = ((), (), s32[]{:S(2)}) async-start(), calls=%async_computation.10 | async-start | bytes 2162688 | tf_op jit(solution)/shard_map/reduce_scatter | solution.py:195
  264.9 16.1 %copy-start.9 = (f32[16,4]{0,1:T(4,128)S(1)}, f32[16,4]{0,1:T(4,128)}, u32[]{:S(2)}) copy-start(f32[16,4]{0,1:T(4,128)} %param.38) | copy-start | bytes 772
  274.3 17.8 %all-to-all-start.2 = ((bf16[16,8,1024]{2,1,0:T(8,128)(2,1)}), bf16[16,8,1024]{2,1,0:T(8,128)(2,1)S(1)}, u32[]{:S(2)}, u32[]{:S(2)}) async-start(bf16[16,8,1024]{2,1,0:T(8,128)(2,1)} %bitcast.96), calls=%async_computation.4 | async-start | bytes 524288 | tf_op jit(solution)/shard_map/all_to_all | solution.py:163
  (3 other events, 6.5 us)
Sparse Core Ops, SparseCore 0:
  27.6 78.4 reduce-scatter.3
  108.8 60.2 all-gather.1
  171.9 15.9 all-reduce.1
  265.0 9.3 reduce-scatter.5
  276.4 139.7 reduce-scatter.7
